TPU v7x, 32 devices: a whole 2x2x4 slice. The times are simulated.
32 devices in a mesh: grp: 2 (over x), tp: 16 (over z, y, core).
Axes of the slice: x: 2, y: 2, z: 4, core: 2. Of those that a mesh axis runs over, the one named last changes fastest.
Arguments:
- tokens: bfloat16 [96, 4096], P('grp', 'tp'), parts along dimension 0, may hold values from -6 to 6
- states: float32 [2, 96, 32, 128, 128], P(None, 'grp', 'tp'), parts along dimension 1, may hold values from -10 to 10
- norm_gain: float32 [2, 4096], replicated, may hold values from 0.1 to 1.9
- query_weight: bfloat16 [2, 4096, 4096], P(None, None, 'tp'), may hold values from -0.09375 to 0.09375
- forget_weight: bfloat16 [2, 4096, 4096], P(None, None, 'tp'), may hold values from -0.09375 to 0.09375
- value_weight: bfloat16 [2, 4096, 4096], P(None, None, 'tp'), may hold values from -0.09375 to 0.09375
- gate_weight: bfloat16 [2, 4096, 4096], P(None, None, 'tp'), may hold values from -0.09375 to 0.09375
- output_weight: bfloat16 [2, 4096, 4096], P(None, 'tp'), may hold values from -0.125 to 0.125
- output_gain: float32 [2, 4096], P(None, 'tp'), may hold values from 0.1 to 1.9
- bound_logits: float32 [4096], P('tp'), may hold values from -6 to 6
Outputs:
- mixed: bfloat16 [96, 4096], P('grp', 'tp'), parts along dimension 0
- new_states: float32 [2, 96, 32, 128, 128], P(None, 'grp', 'tp'), parts along dimension 1
There are 2 independent parts, one for each index of `grp`. A program takes and returns all parts, laid end to end along the dimension named above; an argument that names none is the same for every part. Nothing has to cross between parts.
All inputs are finite; a program needn't handle non-finite values.
Results may differ from a plain program's by a relative error of at most 0.017.
Values may be sent and summed in bfloat16 or wider, within the bound.
A program may use at most 128 MiB of HBM per device.

v0:
```python
import functools

import jax
import jax.numpy as jnp
from jax import lax
from jax.experimental import pallas as pl
from jax.experimental.pallas import tpu as pltpu
from jax.sharding import PartitionSpec as P

epsilon = 1e-06


def kernel(
    n,
    tok,
    states,
    gain,
    wq,
    wf,
    wv,
    wg,
    wo,
    ogain,
    blog,
    mixed,
    new,
    w_s,
    wo_s,
    gain_s,
    ogain_s,
    blog_s,
    xg,
    acc,
    ss,
    tf,
    tq,
    v_s,
    ro_s,
    g_s,
    sb,
    ra,
    pb,
    rb,
    es,
    er,
    ep,
    eb,
    sm_sem,
    w_sem,
    gs,
    gr,
    fs,
    fr,
    asend,
    arecv,
    bsend,
    brecv,
    essend,
    esrecv,
    ebsend,
    ebrecv,
):
    rows, cols = tok.shape
    width = cols * n
    heads = states.shape[2]
    size = states.shape[3]
    groups = rows // 8
    half = n // 2
    me = lax.axis_index("tp")
    sib = me + 1 - 2 * lax.rem(me, 2)

    def peer(s):
        return lax.rem(me + 2 * s, n)

    def origin(s):
        return lax.rem(me - 2 * s + n, n)

    def sib_origin(s):
        return lax.rem(sib - 2 * s + n, n)

    def span(d):
        return pl.ds(pl.multiple_of(d * cols, cols), cols)

    def remote(src, dst, send, recv, d):
        return pltpu.make_async_remote_copy(
            src_ref=src,
            dst_ref=dst,
            send_sem=send,
            recv_sem=recv,
            device_id={"tp": d},
            device_id_type=pl.DeviceIdType.MESH,
        )

    barrier = pltpu.get_barrier_semaphore()

    def greet(d):
        pl.semaphore_signal(
            barrier, inc=1, device_id={"tp": d}, device_id_type=pl.DeviceIdType.MESH
        )

    greet(sib)

    @pl.loop(1, half)
    def _(s):
        greet(peer(s))

    tok_copy = pltpu.make_async_copy(tok, xg.at[0, me], sm_sem.at[0])
    tok_copy.start()
    gain_copy = pltpu.make_async_copy(gain, gain_s, sm_sem.at[1])
    gain_copy.start()
    og_copy = pltpu.make_async_copy(ogain, ogain_s, sm_sem.at[2])
    og_copy.start()
    bl_copy = pltpu.make_async_copy(blog, blog_s, sm_sem.at[3])
    bl_copy.start()

    def weight_copies(l):
        return [
            pltpu.make_async_copy(w.at[l], w_s.at[l, i], w_sem.at[l, i])
            for i, w in enumerate((wq, wf, wv, wg))
        ]

    def later_copies(l):
        return [
            pltpu.make_async_copy(states.at[l], new.at[l], w_sem.at[l, 4]),
            pltpu.make_async_copy(wo.at[l], wo_s.at[l], w_sem.at[l, 5]),
        ]

    for c in weight_copies(0):
        c.start()
    pl.semaphore_wait(barrier, half)
    tok_copy.wait()

    def gather_copy(l, s):
        return remote(xg.at[l, me], xg.at[l, me], gs.at[l, s], gr.at[l, s], peer(s))

    def forward_copy(l, s):
        o = origin(s)
        return remote(xg.at[l, o], xg.at[l, o], fs.at[l, s], fr.at[l, s], sib)

    def a_copy(l, s):
        return remote(sb.at[l, s], ra.at[l, s], asend.at[l, s], arecv.at[l, s], sib)

    def b_copy(l, s):
        return remote(pb.at[l, s], rb.at[l, s], bsend.at[l, s], brecv.at[l, s], peer(s))

    def es_copy(l):
        return remote(es.at[l], er.at[l], essend.at[l], esrecv.at[l], sib)

    def eb_copy(l, s):
        return remote(ep.at[l], eb.at[l, s], ebsend.at[l, s], ebrecv.at[l, s], peer(s))

    for l in range(2):
        forward_copy(l, 0).start()

        @pl.loop(1, half)
        def _(s):
            gather_copy(l, s).start()

        acc[...] = jnp.zeros_like(acc)
        ss[...] = jnp.zeros_like(ss)

        def chunk(o):
            x = xg[l, o].astype(jnp.float32)
            square = x * x
            total = square[:, :128]
            for c in range(128, cols, 128):
                total = total + square[:, c : c + 128]
            ss[...] += total
            scaled = (x * gain_s[l : l + 1, span(o)]).astype(jnp.bfloat16)
            for i in range(4):
                acc[i] += jnp.dot(
                    scaled, w_s[l, i, span(o), :], preferred_element_type=jnp.float32
                )

        if l == 0:
            gain_copy.wait()
        for c in weight_copies(l):
            c.wait()
        if l == 0:
            for c in later_copies(0):
                c.start()
        chunk(me)
        forward_copy(l, 0).wait_recv()
        chunk(sib_origin(0))

        @pl.loop(1, half)
        def _(s):
            gather_copy(l, s).wait_recv()
            forward_copy(l, s).start()
            chunk(origin(s))

        @pl.loop(1, half)
        def _(s):
            forward_copy(l, s).wait_recv()
            chunk(sib_origin(s))

        factor = lax.rsqrt(jnp.sum(ss[...], axis=-1, keepdims=True) / width + epsilon)

        def projected(i):
            return (acc[i] * factor).astype(jnp.bfloat16).astype(jnp.float32)

        if l == 0:
            og_copy.wait()
            bl_copy.wait()
        query = projected(0) * size**-0.5
        forget = jax.nn.sigmoid(projected(1))
        if l == 1:
            lower = jax.nn.sigmoid(blog_s[...])
            forget = lower + (1.0 - lower) * forget
        value = projected(2)
        v_s[...] = value
        kept = query * forget
        fresh = query - kept
        pad = jnp.zeros((size - rows, size), jnp.float32)

        def flip(source, dest):
            for h in range(heads):
                part = source[:, h * size : (h + 1) * size]
                flipped = jnp.concatenate([part, pad], axis=0).T
                for b in range(groups):
                    shift = (size - 8 * b) % size
                    dest[b, h] = pltpu.roll(flipped, shift, 1) if shift else flipped

        flip(kept, tq)
        state_copy, wo_copy = later_copies(l)
        state_copy.wait()

        @pl.loop(0, groups)
        def _(b):
            base = pl.multiple_of(b * 8, 8)
            for h in range(heads):
                lanes = slice(h * size, (h + 1) * size)
                lines = []
                for j in range(8):
                    ask = tq[b, h, :, j : j + 1]
                    lines.append(
                        jnp.sum(ask * new[l, base + j, h], axis=0, keepdims=True)
                    )
                ro_s[pl.ds(base, 8), lanes] = jnp.concatenate(lines, axis=0)

        for h in range(heads):
            lanes = slice(h * size, (h + 1) * size)
            share = jnp.sum(fresh[:, lanes], axis=-1, keepdims=True)
            ro_s[:, lanes] += share * value[:, lanes]

        readout = ro_s[...]
        energy = jnp.sum(readout * readout, axis=-1, keepdims=True)
        lane = lax.broadcasted_iota(jnp.int32, (8, 128), 1)
        tile = jnp.zeros((8, 128), jnp.float32)
        for b in range(groups):
            tile = jnp.where(lane == b, energy[8 * b : 8 * b + 8], tile)
        es[l] = tile
        g_s[...] = (readout * ogain_s[l : l + 1, :] * jax.nn.silu(projected(3))).astype(
            jnp.bfloat16
        )
        es_copy(l).start()
        wo_copy.wait()
        if l == 0:
            for c in weight_copies(1) + later_copies(1):
                c.start()

        def product(d):
            return jnp.dot(
                g_s[...], wo_s[l, :, span(d)], preferred_element_type=jnp.float32
            )

        @pl.loop(0, half)
        def _(t):
            s = lax.rem(t + 1, half)
            sb[l, s] = product(lax.rem(sib + 2 * s, n)).astype(jnp.bfloat16)
            a_copy(l, s).start()

        es_copy(l).wait_recv()
        ep[l] = es[l] + er[l]

        @pl.loop(1, half)
        def _(s):
            eb_copy(l, s).start()
            mine = product(peer(s))
            a_copy(l, s).wait_recv()
            pb[l, s] = (mine + ra[l, s].astype(jnp.float32)).astype(jnp.bfloat16)
            b_copy(l, s).start()

        mine = product(me)
        a_copy(l, 0).wait_recv()
        mine = mine + ra[l, 0].astype(jnp.float32)

        flip(forget, tf)

        @pl.loop(0, groups)
        def _(b):
            base = pl.multiple_of(b * 8, 8)
            for h in range(heads):
                values = v_s[pl.ds(base, 8), h * size : (h + 1) * size]
                for j in range(8):
                    line = values[j : j + 1, :]
                    keep = tf[b, h, :, j : j + 1]
                    new[l, base + j, h] = keep * (new[l, base + j, h] - line) + line

        def collect(s, carry):
            total, powers = carry
            eb_copy(l, s).wait_recv()
            b_copy(l, s).wait_recv()
            return total + rb[l, s].astype(jnp.float32), powers + eb[l, s]

        total, powers = lax.fori_loop(1, half, collect, (mine, ep[l]))
        column = jnp.concatenate([powers[:, b : b + 1] for b in range(groups)], axis=0)
        rescale = lax.rsqrt(column / width + epsilon)
        stream = (xg[l, me].astype(jnp.float32) + total * rescale).astype(jnp.bfloat16)
        if l == 0:
            xg[1, me] = stream
        else:
            mixed[...] = stream

    for l in range(2):
        forward_copy(l, 0).wait_send()
        a_copy(l, 0).wait_send()
        es_copy(l).wait_send()

        @pl.loop(1, half)
        def _(s):
            gather_copy(l, s).wait_send()
            forward_copy(l, s).wait_send()
            a_copy(l, s).wait_send()
            b_copy(l, s).wait_send()
            eb_copy(l, s).wait_send()


def body(
    n,
    tokens,
    states,
    norm_gain,
    query_weight,
    forget_weight,
    value_weight,
    gate_weight,
    output_weight,
    output_gain,
    bound_logits,
):
    rows, cols = tokens.shape
    width = cols * n
    heads, size = states.shape[2:4]
    groups = rows // 8
    half = n // 2
    f32, b16 = jnp.float32, jnp.bfloat16
    dma = pltpu.SemaphoreType.DMA
    anywhere = pl.BlockSpec(memory_space=pl.ANY)
    in_vmem = pl.BlockSpec(memory_space=pltpu.VMEM)
    mixed, new = pl.pallas_call(
        functools.partial(kernel, n),
        out_shape=(
            jax.ShapeDtypeStruct(tokens.shape, b16),
            pltpu.VMEM(states.shape, f32),
        ),
        in_specs=[anywhere] * 10,
        out_specs=(in_vmem, in_vmem),
        scratch_shapes=[
            pltpu.VMEM((2, 4, width, cols), b16),
            pltpu.VMEM((2, cols, width), b16),
            pltpu.VMEM((2, width), f32),
            pltpu.VMEM((2, cols), f32),
            pltpu.VMEM((1, cols), f32),
            pltpu.VMEM((2, n, rows, cols), b16),
            pltpu.VMEM((4, rows, cols), f32),
            pltpu.VMEM((rows, 128), f32),
            pltpu.VMEM((groups, heads, size, size), f32),
            pltpu.VMEM((groups, heads, size, size), f32),
            pltpu.VMEM((rows, cols), f32),
            pltpu.VMEM((rows, cols), f32),
            pltpu.VMEM((rows, cols), b16),
            pltpu.VMEM((2, half, rows, cols), b16),
            pltpu.VMEM((2, half, rows, cols), b16),
            pltpu.VMEM((2, half, rows, cols), b16),
            pltpu.VMEM((2, half, rows, cols), b16),
            pltpu.VMEM((2, 8, 128), f32),
            pltpu.VMEM((2, 8, 128), f32),
            pltpu.VMEM((2, 8, 128), f32),
            pltpu.VMEM((2, half, 8, 128), f32),
            dma((4,)),
            dma((2, 6)),
            dma((2, half)),
            dma((2, half)),
            dma((2, half)),
            dma((2, half)),
            dma((2, half)),
            dma((2, half)),
            dma((2, half)),
            dma((2, half)),
            dma((2,)),
            dma((2,)),
            dma((2, half)),
            dma((2, half)),
        ],
        compiler_params=pltpu.CompilerParams(
            collective_id=0, has_side_effects=True, vmem_limit_bytes=46000 * 1024
        ),
    )(
        tokens,
        states,
        norm_gain,
        query_weight,
        forget_weight,
        value_weight,
        gate_weight,
        output_weight,
        output_gain,
        bound_logits.reshape(1, cols),
    )
    return mixed, new


def solution(mesh):
    placed = (
        P("grp", "tp"),
        P(None, "grp", "tp", None, None),
        P(),
        P(None, None, "tp"),
        P(None, None, "tp"),
        P(None, None, "tp"),
        P(None, None, "tp"),
        P(None, "tp", None),
        P(None, "tp"),
        P("tp"),
    )
    return jax.shard_map(
        functools.partial(body, mesh.shape["tp"]),
        mesh=mesh,
        in_specs=placed,
        out_specs=(P("grp", "tp"), P(None, "grp", "tp", None, None)),
        check_vma=False,
    )
```

profile of v0, /device:TPU:0, one launch (start us, length us, event | category | flops | bytes accessed | tf_op | source)
XLA Modules:
  0.0 52.2 jit_solution(6236378775637316944)
XLA Ops:
  0.6 46.1 %shard_map.113 = (bf16[48,256]{1,0:T(8,128)(2,1)}, f32[2,48,2,128,128]{4,3,2,1,0:T(8,128)S(1)}) custom-call(bf16[48,256]{1,0:T(8,128)(2,1)} %tok.1, f32[2,48,2,128,128]{4,3,2,1,0:T(8,128)} %states.1, f32[2,4096]{1,0:T(2,128)} %gain.1, bf16[2,4096,256]{2,1,0:T(8,128)(2,1)} %wq.1, bf16[2,4096,256]{2,1,0:T(8,128)(2,1)} %wf.1, bf16[2,4096,256]{2,1,0:T(8,128)(2,1)} %wv.1, ...), custom_call_target="tpu_custom_call" | custom-call | tf_op jit(solution)/shard_map/pallas_call | solution.py:351
  46.8 0.0 copy-start
  46.8 4.8 %copy.14 = f32[2,48,2,128,128]{4,3,2,1,0:T(8,128)} copy(f32[2,48,2,128,128]{4,3,2,1,0:T(8,128)S(1)} %get-tuple-element.3) | data formatting | bytes 25165824
  51.6 0.0 copy-done
  51.6 0.6 %copy.15 = bf16[48,256]{1,0:T(8,128)(2,1)} copy(bf16[48,256]{1,0:T(8,128)(2,1)S(1)} %copy-done) | data formatting | bytes 49152
Async XLA Ops:
  46.8 4.8 %copy-start = (bf16[48,256]{1,0:T(8,128)(2,1)S(1)}, bf16[48,256]{1,0:T(8,128)(2,1)}, u32[]{:S(2)}) copy-start(bf16[48,256]{1,0:T(8,128)(2,1)} %get-tuple-element.6) | copy-start | bytes 73732
where the time goes:
time: 52.3 us; the launch traced here: 52.2 us
  Pallas kernels  46.1 us (88%)
  local copies, waits for them, and re-layouts  5.39 us (10%)
  between operations  0.65 us (1%)
    pallas_call x1, Pallas kernels, body(): pl.pallas_call(functools.partial(kernel, n), out_shape=(jax.ShapeDtypeStr...  46.1 us
    unnamed x4, local copies, waits for them, and re-layouts  5.39 us

commit v1 on v0

v1 whole, which is shorter than its diff:
```python
import functools

import jax
import jax.numpy as jnp
from jax import lax
from jax.experimental import pallas as pl
from jax.experimental.pallas import tpu as pltpu
from jax.sharding import PartitionSpec as P

epsilon = 1e-06


def kernel(
    n,
    parts,
    tok,
    states,
    gain,
    wq,
    wf,
    wv,
    wg,
    wo,
    ogain,
    blog,
    mixed,
    new,
    w_s,
    wo_s,
    gain_s,
    ogain_s,
    blog_s,
    xg,
    acc,
    ss,
    tf,
    v_s,
    g_s,
    own,
    sb,
    ra,
    pb,
    rb,
    es,
    er,
    ep,
    eb,
    sm_sem,
    w_sem,
    gs,
    gr,
    fs,
    fr,
    asend,
    arecv,
    bsend,
    brecv,
    essend,
    esrecv,
    ebsend,
    ebrecv,
):
    rows, cols = tok.shape
    width = cols * n
    heads = states.shape[2]
    size = states.shape[3]
    part = rows // parts
    half = n // 2
    bunch = sb.shape[2] // arecv.shape[2]
    f32, b16 = jnp.float32, jnp.bfloat16
    me = lax.axis_index("tp")
    core = lax.rem(me, 2)
    chip = me // 2
    sib = me + 1 - 2 * core

    def other(s):
        found, bit = 0, 1
        while bit < half:
            found = found + bit * ((chip // bit + s // bit) % 2)
            bit *= 2
        return found

    def peer(s):
        return 2 * other(s) + core

    def sib_peer(s):
        return 2 * other(s) + 1 - core

    def span(d):
        return pl.ds(pl.multiple_of(d * cols, cols), cols)

    def lines(p):
        return pl.ds(p * part, part)

    def remote(src, dst, send, recv, d):
        return pltpu.make_async_remote_copy(
            src_ref=src,
            dst_ref=dst,
            send_sem=send,
            recv_sem=recv,
            device_id={"tp": d},
            device_id_type=pl.DeviceIdType.MESH,
        )

    barrier = pltpu.get_barrier_semaphore()

    def greet(d):
        pl.semaphore_signal(
            barrier, inc=1, device_id={"tp": d}, device_id_type=pl.DeviceIdType.MESH
        )

    @pl.loop(1, half)
    def _(t):
        greet(peer(half - t))

    greet(sib)

    tok_copy = pltpu.make_async_copy(tok, xg.at[0, me], sm_sem.at[0])
    tok_copy.start()
    gain_copy = pltpu.make_async_copy(gain, gain_s, sm_sem.at[1])
    gain_copy.start()
    og_copy = pltpu.make_async_copy(ogain, ogain_s, sm_sem.at[2])
    og_copy.start()
    bl_copy = pltpu.make_async_copy(blog, blog_s, sm_sem.at[3])
    bl_copy.start()

    def weight_copies(l):
        return [
            pltpu.make_async_copy(w.at[l], w_s.at[l, i], w_sem.at[l, i])
            for i, w in enumerate((wq, wf, wv, wg))
        ]

    def later_copies(l):
        return [
            pltpu.make_async_copy(states.at[l], new.at[l], w_sem.at[l, 4]),
            pltpu.make_async_copy(wo.at[l], wo_s.at[l], w_sem.at[l, 5]),
        ]

    for c in weight_copies(0):
        c.start()
    tok_copy.wait()
    pl.semaphore_wait(barrier, half)

    def gather_copy(l, s):
        return remote(xg.at[l, me], xg.at[l, me], gs.at[l], gr.at[l, s], peer(s))

    def gather_part(l, p, s):
        ref = xg.at[l, me, lines(p)]
        return remote(ref, ref, gs.at[l], gr.at[l, s], peer(s))

    def forward_copy(l, s):
        o = peer(s)
        return remote(xg.at[l, o], xg.at[l, o], fs.at[l], fr.at[l, s], sib)

    def a_copy(l, p, c):
        block = pl.ds(c * bunch, bunch)
        return remote(
            sb.at[l, p, block],
            ra.at[l, p, block],
            asend.at[l],
            arecv.at[l, p, c],
            sib,
        )

    def b_copy(l, p, i):
        d = peer(half - 1 - i)
        return remote(
            pb.at[l, p, i], rb.at[l, p, i], bsend.at[l], brecv.at[l, p], d
        )

    def es_copy(l, p):
        return remote(
            es.at[l, p], er.at[l, p], essend.at[l, p], esrecv.at[l, p], sib
        )

    def eb_copy(l, p, i):
        d = peer(half - 1 - i)
        return remote(ep.at[l, p], eb.at[l, p, i], ebsend.at[l], ebrecv.at[l, p], d)

    row_of = lax.broadcasted_iota(jnp.int32, (part, 128), 0)
    diagonal = row_of == lax.broadcasted_iota(jnp.int32, (part, 128), 1)

    @pl.loop(1, half)
    def _(t):
        gather_copy(0, half - t).start()

    forward_copy(0, 0).start()

    for l in range(2):
        acc[...] = jnp.zeros_like(acc)
        ss[...] = jnp.zeros_like(ss)

        def chunk(o):
            x = xg[l, o].astype(f32)
            square = x * x
            total = square[:, :128]
            for c in range(128, cols, 128):
                total = total + square[:, c : c + 128]
            ss[...] += total
            scaled = (x * gain_s[l : l + 1, span(o)]).astype(b16)
            for i in range(4):
                acc[i] += jnp.dot(
                    scaled, w_s[l, i, span(o), :], preferred_element_type=f32
                )

        if l == 0:
            gain_copy.wait()
        for c in weight_copies(l):
            c.wait()
        if l == 0:
            for c in later_copies(0):
                c.start()
        chunk(me)
        forward_copy(l, 0).wait_recv()
        chunk(sib)

        @pl.loop(1, half)
        def _(s):
            gather_copy(l, s).wait_recv()
            forward_copy(l, s).start()
            chunk(peer(s))

        @pl.loop(1, half)
        def _(s):
            forward_copy(l, s).wait_recv()
            chunk(sib_peer(s))

        factor = lax.rsqrt(jnp.sum(ss[...], axis=-1, keepdims=True) / width + epsilon)

        def projected(i):
            return (acc[i] * factor).astype(b16).astype(f32)

        if l == 0:
            og_copy.wait()
            bl_copy.wait()
        query = projected(0) * size**-0.5
        forget = jax.nn.sigmoid(projected(1))
        if l == 1:
            lower = jax.nn.sigmoid(blog_s[...])
            forget = lower + (1.0 - lower) * forget
        value = projected(2)
        v_s[...] = value
        kept = query * forget
        fresh = query - kept
        gate = ogain_s[l : l + 1, :] * jax.nn.silu(projected(3))
        pad = jnp.zeros((size - rows, size), f32)
        state_copy, wo_copy = later_copies(l)
        state_copy.wait()
        wo_copy.wait()
        if l == 0:
            for c in weight_copies(1) + later_copies(1):
                c.start()

        for p in range(parts):
            here = slice(p * part, (p + 1) * part)
            reads = []
            for h in range(heads):
                lanes = slice(h * size, (h + 1) * size)
                asked = kept[here, lanes]
                spread = jnp.concatenate(
                    [
                        jnp.where(row_of == j, asked, 0.0).astype(b16)
                        for j in range(part)
                    ],
                    axis=1,
                )
                held = new[l, here, h].reshape(part * size, size).astype(b16)
                old = jnp.dot(spread, held, preferred_element_type=f32)
                share = jnp.sum(fresh[here, lanes], axis=-1, keepdims=True)
                reads.append(old + share * value[here, lanes])
            readout = jnp.concatenate(reads, axis=1)
            energy = jnp.sum(readout * readout, axis=-1, keepdims=True)
            es[l, p] = jnp.sum(
                jnp.where(diagonal, energy, 0.0), axis=0, keepdims=True
            )
            es_copy(l, p).start()
            g_s[here, :] = (readout * gate[here, :]).astype(b16)

            def product(d):
                return jnp.dot(
                    g_s[here, :], wo_s[l, :, span(d)], preferred_element_type=f32
                )

            @pl.loop(0, half // bunch)
            def _(c):
                for k in range(bunch):
                    i = c * bunch + k
                    sb[l, p, i] = product(sib_peer(half - 1 - i)).astype(b16)
                a_copy(l, p, c).start()

            es_copy(l, p).wait_recv()
            ep[l, p] = es[l, p] + er[l, p]

            @pl.loop(0, half // bunch)
            def _(c):
                mine = [
                    product(peer(half - 1 - c * bunch - k)) for k in range(bunch)
                ]
                a_copy(l, p, c).wait_recv()
                for k in range(bunch):
                    i = c * bunch + k
                    both = mine[k] + ra[l, p, i].astype(f32)
                    if k < bunch - 1:
                        pb[l, p, i] = both.astype(b16)
                        b_copy(l, p, i).start()
                        eb_copy(l, p, i).start()
                    else:
                        own[p] = both

                        @pl.when(c < half // bunch - 1)
                        def _():
                            pb[l, p, i] = own[p].astype(b16)
                            b_copy(l, p, i).start()
                            eb_copy(l, p, i).start()

        for h in range(heads):
            lane = slice(h * size, (h + 1) * size)
            flipped = jnp.concatenate([forget[:, lane], pad], axis=0).T
            for b in range(rows // 8):
                shift = (size - 8 * b) % size
                tf[b, h] = pltpu.roll(flipped, shift, 1) if shift else flipped

        def update(first, last):
            @pl.loop(first, last)
            def _(b):
                base = pl.multiple_of(b * 8, 8)
                for h in range(heads):
                    values = v_s[pl.ds(base, 8), h * size : (h + 1) * size]
                    for j in range(8):
                        line = values[j : j + 1, :]
                        keep = tf[b, h, :, j : j + 1]
                        new[l, base + j, h] = (
                            keep * (new[l, base + j, h] - line) + line
                        )

        if l == 1:
            update(0, rows // 8)

        for p in range(parts):
            here = slice(p * part, (p + 1) * part)
            remote(
                ep.at[l, p], eb.at[l, p], ebsend.at[l], ebrecv.at[l, p], sib
            ).wait_recv()
            powers = ep[l, p]
            for i in range(half - 1):
                powers = powers + eb[l, p, i]
            column = jnp.sum(
                jnp.where(diagonal, powers, 0.0), axis=1, keepdims=True
            )
            rescale = lax.rsqrt(column / width + epsilon)
            remote(
                pb.at[l, p], rb.at[l, p], bsend.at[l], brecv.at[l, p], sib
            ).wait_recv()
            total = own[p]
            for i in range(half - 1):
                total = total + rb[l, p, i].astype(f32)
            stream = (xg[l, me, here].astype(f32) + total * rescale).astype(b16)
            if l == 0:
                xg[1, me, here] = stream

                @pl.loop(1, half)
                def _(t):
                    gather_part(1, p, half - t).start()

                if p == parts - 1:
                    forward_copy(1, 0).start()
                update(p * part // 8, (p + 1) * part // 8)
            else:
                mixed[here, :] = stream

    for l in range(2):
        remote(
            xg.at[l, pl.ds(0, half - 1)],
            xg.at[l, pl.ds(0, half - 1)],
            gs.at[l],
            gr.at[l, 0],
            sib,
        ).wait_send()
        remote(
            xg.at[l, pl.ds(0, half)],
            xg.at[l, pl.ds(0, half)],
            fs.at[l],
            fr.at[l, 0],
            sib,
        ).wait_send()
        remote(sb.at[l], ra.at[l], asend.at[l], arecv.at[l, 0, 0], sib).wait_send()
        remote(pb.at[l], rb.at[l], bsend.at[l], brecv.at[l, 0], sib).wait_send()
        remote(eb.at[l], eb.at[l], ebsend.at[l], ebrecv.at[l, 0], sib).wait_send()
        for p in range(parts):
            es_copy(l, p).wait_send()


def body(
    n,
    tokens,
    states,
    norm_gain,
    query_weight,
    forget_weight,
    value_weight,
    gate_weight,
    output_weight,
    output_gain,
    bound_logits,
):
    rows, cols = tokens.shape
    width = cols * n
    heads, size = states.shape[2:4]
    groups = rows // 8
    half = n // 2
    bunch = 4
    parts = rows // 16
    part = rows // parts
    f32, b16 = jnp.float32, jnp.bfloat16
    dma = pltpu.SemaphoreType.DMA
    anywhere = pl.BlockSpec(memory_space=pl.ANY)
    in_vmem = pl.BlockSpec(memory_space=pltpu.VMEM)
    mixed, new = pl.pallas_call(
        functools.partial(kernel, n, parts),
        out_shape=(
            jax.ShapeDtypeStruct(tokens.shape, b16),
            pltpu.VMEM(states.shape, f32),
        ),
        in_specs=[anywhere] * 10,
        out_specs=(in_vmem, in_vmem),
        scratch_shapes=[
            pltpu.VMEM((2, 4, width, cols), b16),
            pltpu.VMEM((2, cols, width), b16),
            pltpu.VMEM((2, width), f32),
            pltpu.VMEM((2, cols), f32),
            pltpu.VMEM((1, cols), f32),
            pltpu.VMEM((2, n, rows, cols), b16),
            pltpu.VMEM((4, rows, cols), f32),
            pltpu.VMEM((rows, 128), f32),
            pltpu.VMEM((groups, heads, size, size), f32),
            pltpu.VMEM((rows, cols), f32),
            pltpu.VMEM((rows, cols), b16),
            pltpu.VMEM((parts, part, cols), f32),
            pltpu.VMEM((2, parts, half, part, cols), b16),
            pltpu.VMEM((2, parts, half, part, cols), b16),
            pltpu.VMEM((2, parts, half - 1, part, cols), b16),
            pltpu.VMEM((2, parts, half - 1, part, cols), b16),
            pltpu.VMEM((2, parts, 1, 128), f32),
            pltpu.VMEM((2, parts, 1, 128), f32),
            pltpu.VMEM((2, parts, 1, 128), f32),
            pltpu.VMEM((2, parts, half - 1, 1, 128), f32),
            dma((4,)),
            dma((2, 6)),
            dma((2,)),
            dma((2, half)),
            dma((2,)),
            dma((2, half)),
            dma((2,)),
            dma((2, parts, half // bunch)),
            dma((2,)),
            dma((2, parts)),
            dma((2, parts)),
            dma((2, parts)),
            dma((2,)),
            dma((2, parts)),
        ],
        compiler_params=pltpu.CompilerParams(
            collective_id=0, has_side_effects=True, vmem_limit_bytes=46000 * 1024
        ),
    )(
        tokens,
        states,
        norm_gain,
        query_weight,
        forget_weight,
        value_weight,
        gate_weight,
        output_weight,
        output_gain,
        bound_logits.reshape(1, cols),
    )
    return mixed, new


def solution(mesh):
    placed = (
        P("grp", "tp"),
        P(None, "grp", "tp", None, None),
        P(),
        P(None, None, "tp"),
        P(None, None, "tp"),
        P(None, None, "tp"),
        P(None, None, "tp"),
        P(None, "tp", None),
        P(None, "tp"),
        P("tp"),
    )
    return jax.shard_map(
        functools.partial(body, mesh.shape["tp"]),
        mesh=mesh,
        in_specs=placed,
        out_specs=(P("grp", "tp"), P(None, "grp", "tp", None, None)),
        check_vma=False,
    )
```

time: 52.3 us -> 47.2 us (0.902)
  Pallas kernels: 46.1 us -> 41 us
    pallas_call x1, Pallas kernels: 46.1 us -> 41 us  [body(): pl.pallas_call(functools.partial(kernel, n, parts), out_shape=(jax.ShapeD...]
where the time goes in v1:
time: 47.2 us; the launch traced here: 47.1 us
  Pallas kernels  41 us (87%)
  local copies, waits for them, and re-layouts  5.39 us (11%)
  between operations  0.65 us (1%)
    pallas_call x1, Pallas kernels, body(): pl.pallas_call(functools.partial(kernel, n, parts), out_shape=(jax.ShapeD...  41 us
    unnamed x4, local copies, waits for them, and re-layouts  5.39 us

profile of v1, /device:TPU:0, one launch (start us, length us, event | category | flops | bytes accessed | tf_op | source)
XLA Modules:
  0.0 47.1 jit_solution(16200945880047040153)
XLA Ops:
  0.6 41.0 %shard_map.113 = (bf16[48,256]{1,0:T(8,128)(2,1)}, f32[2,48,2,128,128]{4,3,2,1,0:T(8,128)S(1)}) custom-call(bf16[48,256]{1,0:T(8,128)(2,1)} %tok.1, f32[2,48,2,128,128]{4,3,2,1,0:T(8,128)} %states.1, f32[2,4096]{1,0:T(2,128)} %gain.1, bf16[2,4096,256]{2,1,0:T(8,128)(2,1)} %wq.1, bf16[2,4096,256]{2,1,0:T(8,128)(2,1)} %wf.1, bf16[2,4096,256]{2,1,0:T(8,128)(2,1)} %wv.1, ...), custom_call_target="tpu_custom_call" | custom-call | tf_op jit(solution)/shard_map/pallas_call | solution.py:418
  41.7 0.0 copy-start
  41.7 4.8 %copy.14 = f32[2,48,2,128,128]{4,3,2,1,0:T(8,128)} copy(f32[2,48,2,128,128]{4,3,2,1,0:T(8,128)S(1)} %get-tuple-element.3) | data formatting | bytes 25165824
  46.5 0.0 copy-done
  46.5 0.6 %copy.15 = bf16[48,256]{1,0:T(8,128)(2,1)} copy(bf16[48,256]{1,0:T(8,128)(2,1)S(1)} %copy-done) | data formatting | bytes 49152
Async XLA Ops:
  41.7 4.8 %copy-start = (bf16[48,256]{1,0:T(8,128)(2,1)S(1)}, bf16[48,256]{1,0:T(8,128)(2,1)}, u32[]{:S(2)}) copy-start(bf16[48,256]{1,0:T(8,128)(2,1)} %get-tuple-element.6) | copy-start | bytes 73732
